TPU v7x, 32 devices: a whole 2x2x4 slice. The times are simulated.
32 devices in a mesh: sp: 8 (over z, y), tp: 4 (over x, core).
Axes of the slice: x: 2, y: 2, z: 4, core: 2. Of those that a mesh axis runs over, the one named last changes fastest.
Arguments:
- resid_in: bfloat16 [2048, 2048], P('sp'), may hold values from -6 to 6
- query_latent: bfloat16 [2048, 768], P('sp'), may hold values from -6 to 6
- kv_latent: bfloat16 [2048, 512], P('sp'), may hold values from -6 to 6
- rotary_key: bfloat16 [2048, 64], P('sp'), may hold values from -200 to 200
- query_gain: float32 [768], replicated, may hold values from 0.1 to 1.9
- kv_gain: float32 [512], replicated, may hold values from 0.1 to 1.9
- w_query_plain: bfloat16 [768, 2048], P(None, 'tp'), may hold values from -0.875 to 0.875
- w_query_rotary: bfloat16 [768, 1024], P(None, 'tp'), may hold values from -0.875 to 0.875
- w_key_plain: bfloat16 [512, 2048], P(None, 'tp'), may hold values from -0.25 to 0.25
- w_value: bfloat16 [512, 2048], P(None, 'tp'), may hold values from -0.25 to 0.25
- w_output: bfloat16 [2048, 2048], P('tp'), may hold values from -0.125 to 0.125
- ffn_gain: float32 [2048], replicated, may hold values from 0.1 to 1.9
- w_gate: bfloat16 [2048, 5632], P('sp', 'tp'), may hold values from -0.125 to 0.125
- w_up: bfloat16 [2048, 5632], P('sp', 'tp'), may hold values from -0.125 to 0.125
- w_down: bfloat16 [5632, 2048], P('tp', 'sp'), may hold values from -0.078125 to 0.078125
Outputs:
- resid_out: bfloat16 [2048, 2048], P(('sp', 'tp'))
All inputs are finite; a program needn't handle non-finite values.
Results may differ from a plain program's by a relative error of at most 0.014.
The roundings to bfloat16 on the way count: a program that leaves them out, or rounds other values in their place, can miss the bound.
Values may be sent and summed in bfloat16 or wider, within the bound.
No kernel may reach another device: no remote copies, remote signals or barrier semaphores. Data moves between devices by JAX's collectives and lax.ppermute only.
A program may use at most 192 MiB of HBM per device.

v0:
```python
import functools

import jax
import jax.numpy as jnp
from jax import lax
from jax.experimental import pallas as pl
from jax.experimental.pallas import tpu as pltpu
from jax.sharding import PartitionSpec as P


NOPE = 128
ROPE = 64
VDIM = 128
EPS = 1e-06


F32 = jnp.float32
BF16 = jnp.bfloat16
NT = (((1,), (1,)), ((), ()))
NN = (((1,), (0,)), ((), ()))


def mm(a, b, dims=NN):
    return lax.dot_general(a, b, dims, preferred_element_type=F32)


def normed(values, gain):
    wide = values.astype(F32)
    return wide * lax.rsqrt(jnp.mean(wide * wide, axis=-1, keepdims=True) + EPS) * gain


def attention_kernel(n, half, first, t_ref, qp_ref, qr_ref, wk_ref, wv_ref, *rest):
    if first:
        pieces = rest[:n]
        top_ref, total_ref, acc_ref = rest[n : n + 3]
    else:
        top_in, total_in, acc_in, wo_ref = rest[:4]
        rest = rest[4:]
        pieces = rest[:n]
        own_ref, core_ref, side_ref, cross_ref = rest[n : n + 4]
        out_ref = rest[-1]
        rest = rest[:-1]
    k_ref, v_ref, r_ref = rest[-4:-1]
    attn_ref = rest[-1]
    width = wk_ref.shape[0]
    rows = ROPE * half // width
    for i, piece in enumerate(pieces):
        lat = piece[:half, :]
        at = pl.ds(i * half, half)
        k_ref[at, :] = mm(lat, wk_ref[...]).astype(BF16)
        v_ref[at, :] = mm(lat, wv_ref[...]).astype(BF16)
        for b in range(width // half):
            r_ref[pl.ds(b * rows, rows), at] = piece[half : half + rows, b * half : (b + 1) * half]
    scale = (NOPE + ROPE) ** (-0.5)
    heads = wk_ref.shape[1] // NOPE
    for h in range(heads):
        lane = slice(h * NOPE, (h + 1) * NOPE)
        score = mm(qp_ref[:, lane], k_ref[:, lane], NT)
        score = (score + mm(qr_ref[:, h * ROPE : (h + 1) * ROPE], r_ref[...])) * scale
        top = jnp.max(score, axis=-1, keepdims=True)
        if not first:
            before = top_in[:, h * NOPE : h * NOPE + 1]
            top = jnp.maximum(top, before)
        weight = jnp.exp(score - top)
        total = jnp.sum(weight, axis=-1, keepdims=True)
        mixed = mm(weight.astype(BF16), v_ref[:, lane])
        if first:
            top_ref[:, lane] = jnp.broadcast_to(top, mixed.shape)
            total_ref[:, lane] = jnp.broadcast_to(total, mixed.shape)
            acc_ref[:, lane] = mixed
        else:
            fade = jnp.exp(before - top)
            total = total + fade * total_in[:, h * NOPE : h * NOPE + 1]
            mixed = mixed + fade * acc_in[:, lane]
            attn_ref[:, lane] = (mixed / total).astype(BF16)
    if first:
        return
    out_ref[...] = mm(attn_ref[...], wo_ref[...])
    share = out_ref.shape[0] // 4
    t = t_ref[0]

    def rows(flip):
        return out_ref[pl.ds(pl.multiple_of((t ^ flip) * share, share), share), :]

    own_ref[...] = rows(0)
    core_ref[...] = rows(1).astype(BF16)
    side_ref[...] = rows(2).astype(BF16)
    cross_ref[...] = rows(3).astype(BF16)


def ffn_kernel(n_tok, n_blk, fcols, b_ref, *rest):
    tok = rest[:n_tok]
    blocks = rest[n_tok : n_tok + n_blk]
    own_ref, other_ref, h_ref = rest[n_tok + n_blk :]
    share = tok[0].shape[0]
    for i, t in enumerate(tok):
        h_ref[i * share : (i + 1) * share, :] = t[...]
    width = blocks[0].shape[1]
    count = n_tok * share
    gate = jnp.zeros((count, fcols), F32)
    upper = jnp.zeros((count, fcols), F32)
    for i, w in enumerate(blocks):
        part = h_ref[:, pl.ds(pl.multiple_of(b_ref[i] * width, width), width)]
        gate = gate + mm(part, w[:fcols, :], NT)
        upper = upper + mm(part, w[fcols : 2 * fcols, :], NT)
    hidden = (gate * jax.nn.sigmoid(gate) * upper).astype(BF16)
    mid = count // 2
    for i, w in enumerate(blocks):
        at = pl.ds(pl.multiple_of(b_ref[i] * width, width), width)
        out = mm(hidden, w[2 * fcols :, :])
        own_ref[:, at] = out[:mid]
        other_ref[:, at] = out[mid:].astype(BF16)


def vmem(n):
    return [pl.BlockSpec(memory_space=pltpu.VMEM)] * n


def small(mib):
    return min(mib, 56) << 20


SMEM = pl.BlockSpec(memory_space=pltpu.SMEM)


def make(mesh):
    n_sp, n_tp = mesh.shape["sp"], mesh.shape["tp"]
    nz = 4
    ny = n_sp // nz
    nc = 2
    nx = n_tp // nc

    def permute(value, dz=0, dy=0, dx=0, dc=0):
        pairs = []
        for s in range(n_sp):
            for t in range(n_tp):
                z, y = divmod(s, ny)
                x, c = divmod(t, nc)
                s2 = (z ^ dz) * ny + (y + dy) % ny
                t2 = (x + dx) % nx * nc + (c + dc) % nc
                pairs.append((s * n_tp + t, s2 * n_tp + t2))
        return lax.ppermute(value, ("sp", "tp"), pairs)

    def shards(
        resid_in,
        query_latent,
        kv_latent,
        rotary_key,
        query_gain,
        kv_gain,
        w_query_plain,
        w_query_rotary,
        w_key_plain,
        w_value,
        w_output,
        ffn_gain,
        w_gate,
        w_up,
        w_down,
    ):
        tok, width = resid_in.shape
        kvr = kv_latent.shape[1]
        heads = w_query_plain.shape[1] // NOPE
        s_id = lax.axis_index("sp")
        t_id = lax.axis_index("tp")
        z, y = s_id // ny, s_id % ny
        c = t_id % nc
        position = (s_id * tok + jnp.arange(tok, dtype=jnp.int32)).astype(F32)
        freq = 10000.0 ** (-jnp.arange(0, ROPE, 2, dtype=F32) / ROPE)
        angle = position[:, None] * freq[None, :]
        cosine = jnp.cos(angle)
        sine = jnp.sin(angle)

        half = tok // nc
        lat = normed(lax.dynamic_slice_in_dim(kv_latent, c * half, half, 0), kv_gain).astype(BF16)
        key = lax.dynamic_slice_in_dim(rotary_key, c * half, half, 0).astype(F32)
        cos_k = lax.dynamic_slice_in_dim(cosine, c * half, half, 0)
        sin_k = lax.dynamic_slice_in_dim(sine, c * half, half, 0)
        ka, kb = key[:, : ROPE // 2], key[:, ROPE // 2 :]
        rot = jnp.concatenate([ka * cos_k - kb * sin_k, kb * cos_k + ka * sin_k], axis=1)
        rot = rot.astype(BF16).T
        per = kvr // half
        rows = ROPE // per
        rot = jnp.concatenate([rot[b * rows : (b + 1) * rows] for b in range(per)], axis=1)
        piece = jnp.concatenate([lat, rot], axis=0)
        kv = [piece] + [permute(piece, dz=i) for i in range(1, nz)]
        far = [permute(p, dy=j) for j in range(1, ny) for p in kv]
        near = [permute(p, dc=1) for p in kv]
        cross = [permute(p, dc=1) for p in far]

        fcols = w_gate.shape[1] // nz
        wg = w_gate.T.reshape(nz, fcols, -1)
        wu = w_up.T.reshape(nz, fcols, -1)
        wd = w_down.reshape(nz, fcols, -1)
        packed = jnp.concatenate([wg, wu, wd], axis=1)

        def weights_for(i):
            return lax.dynamic_index_in_dim(packed, z ^ i, 0, keepdims=False)

        weights, blocks = [], []
        for i in range(nz):
            held = permute(weights_for(i), dz=i) if i else weights_for(0)
            weights.append(held)
            blocks.append((z ^ i) * ny + y)
            for j in range(1, ny):
                weights.append(permute(held, dy=j))
                blocks.append((z ^ i) * ny + (y - j) % ny)
        if weights[0].shape[1] % 128:
            place = (y - jnp.arange(ny)) % ny

            def merged(group):
                joined = []
                for i in range(nz):
                    stacked = jnp.stack(group[i * ny : (i + 1) * ny])[place]
                    joined.append(jnp.moveaxis(stacked, 0, 1).reshape(stacked.shape[1], -1))
                return joined

            weights = merged(weights)
            blocks = [z ^ i for i in range(nz)]
        blocks = jnp.stack(blocks).astype(jnp.int32)

        q_norm = normed(query_latent, query_gain).astype(BF16)
        q_plain = mm(q_norm, w_query_plain).astype(BF16)
        q_raw = mm(q_norm, w_query_rotary).reshape(tok, heads, ROPE)
        qa, qb = q_raw[..., : ROPE // 2], q_raw[..., ROPE // 2 :]
        cos_q, sin_q = cosine[:, None, :], sine[:, None, :]
        q_rot = jnp.concatenate([qa * cos_q - qb * sin_q, qb * cos_q + qa * sin_q], axis=-1)
        q_rot = q_rot.astype(BF16).reshape(tok, heads * ROPE)

        share = tok // n_tp
        t32 = t_id[None].astype(jnp.int32)
        wide = heads * NOPE
        near, far = kv + near, far + cross

        def attend(first, pieces, *extra):
            n = len(pieces)
            share = tok // n_tp
            if first:
                shapes = (jax.ShapeDtypeStruct((tok, wide), F32),) * 3
            else:
                shapes = (jax.ShapeDtypeStruct((share, width), F32),)
                shapes = shapes + (jax.ShapeDtypeStruct((share, width), BF16),) * 3
            return pl.pallas_call(
                functools.partial(attention_kernel, n, half, first),
                out_shape=shapes,
                in_specs=[SMEM] + vmem(4 + len(extra) + n),
                out_specs=tuple(vmem(len(shapes))),
                scratch_shapes=[
                    pltpu.VMEM((n * half, wide), BF16),
                    pltpu.VMEM((n * half, heads * VDIM), BF16),
                    pltpu.VMEM((ROPE, n * half), BF16),
                    pltpu.VMEM((tok, heads * VDIM), BF16),
                ]
                + ([] if first else [pltpu.VMEM((tok, width), F32)]),
                compiler_params=pltpu.CompilerParams(vmem_limit_bytes=small(12 + n)),
                name="attention",
            )(t32, q_plain, q_rot, w_key_plain, w_value, *extra, *pieces)

        share = tok // n_tp
        resid = lax.dynamic_slice_in_dim(resid_in, t_id * share, share, 0)
        stats = attend(True, near)
        own, core, side, cross = attend(False, far, *stats, w_output)
        side = permute(side, dx=1)
        cross = permute(cross, dx=1, dc=1)
        core = permute(core, dc=1)
        summed = (own + core.astype(F32)) + (side.astype(F32) + cross.astype(F32))
        mid = resid.astype(F32) + summed
        h_norm = normed(mid, ffn_gain).astype(BF16)

        nb = len(blocks)

        def reduced(i):
            tokens = sides[i][0] + sides[i][1]
            count = len(tokens) * share
            own, other = pl.pallas_call(
                functools.partial(ffn_kernel, len(tokens), nb, fcols),
                out_shape=(
                    jax.ShapeDtypeStruct((count // nc, width), F32),
                    jax.ShapeDtypeStruct((count // nc, width), BF16),
                ),
                in_specs=[SMEM] + vmem(len(tokens) + nb),
                out_specs=tuple(vmem(2)),
                scratch_shapes=[pltpu.VMEM((count, width), BF16)],
                compiler_params=pltpu.CompilerParams(vmem_limit_bytes=small(14)),
                name="ffn",
            )(blocks, *tokens, *weights)
            return own + permute(other, dc=1).astype(F32)

        def halved(chip):
            back = permute(chip[share:].astype(BF16), dx=1)
            return chip[:share] + back.astype(F32)

        opposite = permute(h_norm, dz=3)
        held = [h_norm, permute(h_norm, dz=1), permute(opposite, dz=1), opposite]
        across = [permute(held[0], dx=1)]
        across.append(permute(across[0], dz=1))
        across = across + [permute(held[i], dx=1) for i in range(2, nz)]
        sides = []
        for i in range(nz):
            near = [permute(held[i], dc=1), permute(across[i], dc=1)]
            sides.append(([held[i], across[i]], near))
        chip = reduced(0) + permute(reduced(1).astype(BF16), dz=1).astype(F32)
        out = mid + halved(chip)
        passed = permute(halved(reduced(3)).astype(BF16), dz=1).astype(F32)
        block = (halved(reduced(2)) + passed).astype(BF16)
        out = out + permute(block, dz=2).astype(F32)
        return out.astype(BF16)

    return shards


def solution(mesh):
    return jax.shard_map(
        make(mesh),
        mesh=mesh,
        in_specs=(
            P("sp", None),
            P("sp", None),
            P("sp", None),
            P("sp", None),
            P(),
            P(),
            P(None, "tp"),
            P(None, "tp"),
            P(None, "tp"),
            P(None, "tp"),
            P("tp", None),
            P(),
            P("sp", "tp"),
            P("sp", "tp"),
            P("tp", "sp"),
        ),
        out_specs=P(("sp", "tp"), None),
        check_vma=False,
    )
```

profile of v0, /device:TPU:0, one launch (start us, length us, event | category | flops | bytes accessed | tf_op | source)
XLA Modules:
  0.0 187.1 jit_solution(16367460703173118846)
XLA Ops:
  3.2 3.1 %collective-permute-start = (bf16[144,512]{1,0:T(8,128)(2,1)S(1)}, bf16[144,512]{1,0:T(8,128)(2,1)S(1)}, u32[]{:S(2)}, u32[]{:S(2)}) collective-permute-start(bf16[144,512]{1,0:T(8,128)(2,1)S(1)} %maximum_maximum_fusion.rest_0_), channel_id=1, source_target_pairs={{0,8},{1,9},{2,10},{3,11},{4,12},{5,13},{6,14},{7,15},{8,0},{9,1},... | collective-permute-start | bytes 442376 | tf_op jit(solution)/shard_map/ppermute | solution.py:142
  6.3 2.6 %collective-permute-start.1 = (bf16[144,512]{1,0:T(8,128)(2,1)S(1)}, bf16[144,512]{1,0:T(8,128)(2,1)S(1)}, u32[]{:S(2)}, u32[]{:S(2)}) collective-permute-start(bf16[144,512]{1,0:T(8,128)(2,1)S(1)} %maximum_maximum_fusion.rest_0_), channel_id=1, source_target_pairs={{0,16},{1,17},{2,18},{3,19},{4,20},{5,21},{6,22},{7,23},{8,24},{9,... | collective-permute-start | bytes 442376 | tf_op jit(solution)/shard_map/ppermute | solution.py:142
  13.2 2.2 %copy.25 = bf16[256,1408]{0,1:T(8,128)(2,1)} copy(bf16[256,1408]{1,0:T(8,128)(2,1)} %param.28) | data formatting | bytes 1441792 | tf_op args[13]
  15.4 2.9 %pad_maximum_fusion = bf16[4,1056,256]{2,1,0:T(8,128)(2,1)} fusion(bf16[4,352,256]{2,1,0:T(8,128)(2,1)} %bitcast.32, bf16[4,352,256]{2,1,0:T(8,128)(2,1)} %bitcast.31, bf16[4,352,256]{2,1,0:T(8,128)(2,1)S(1)} %bitcast.30), kind=kLoop, calls=%fused_computation | loop fusion | flops 6488064 | bytes 4325376 | tf_op jit(solution)/shard_map/concatenate | solution.py:195
  26.3 2.8 %collective-permute-done.9.rest_6_ = bf16[144,512]{1,0:T(8,128)(2,1)S(1)} collective-permute-done((bf16[144,512]{1,0:T(8,128)(2,1)S(1)}, bf16[144,512]{1,0:T(8,128)(2,1)S(1)}, u32[]{:S(2)}, u32[]{:S(2)}) %collective-permute-start.9) | collective-permute-done | bytes 147488 | tf_op jit(solution)/shard_map/ppermute | solution.py:142
  29.1 2.6 %collective-permute-done.10.rest_7_ = bf16[144,512]{1,0:T(8,128)(2,1)S(1)} collective-permute-done((bf16[144,512]{1,0:T(8,128)(2,1)S(1)}, bf16[144,512]{1,0:T(8,128)(2,1)S(1)}, u32[]{:S(2)}, u32[]{:S(2)}) %collective-permute-start.10) | collective-permute-done | bytes 147488 | tf_op jit(solution)/shard_map/ppermute | solution.py:142
  33.1 4.7 %attention.2 = (f32[256,512]{1,0:T(8,128)S(1)}, f32[256,512]{1,0:T(8,128)S(1)}, f32[256,512]{1,0:T(8,128)S(1)}) custom-call(s32[1]{0:T(128)} %bitcast.t_ref, bf16[256,512]{1,0:T(8,128)(2,1)S(1)} %convolution_convert_fusion.qp_ref, bf16[256,256]{1,0:T(8,128)(2,1)S(1)} %copy.23.qr_ref, bf16[512,512]{1,0:T(8,128)(2,1)S(1)} %copy-done.2, ...), custom_call_target="tpu_custom_call" | custom-call | tf_op jit(solution)/shard_map/attention/pallas_call | solution.py:243
  37.9 5.7 %attention.3 = (f32[64,2048]{1,0:T(8,128)S(1)}, bf16[64,2048]{1,0:T(8,128)(2,1)S(1)}, bf16[64,2048]{1,0:T(8,128)(2,1)}, bf16[64,2048]{1,0:T(8,128)(2,1)}) custom-call(s32[1]{0:T(128)} %bitcast.t_ref, bf16[256,512]{1,0:T(8,128)(2,1)S(1)} %convolution_convert_fusion.qp_ref, bf16[256,256]{1,0:T(8,128)(2,1)S(1)} %copy.23.qr_ref, bf16[512,512]{1,0:T(8,128)(2,1)S(1)} %copy-done.2, ...), custom_call_target="tpu_custom_call" | custom-call | tf_op jit(solution)/shard_map/attention/pallas_call | solution.py:243
  47.3 3.5 %collective-permute-start.24 = (bf16[1056,256]{1,0:T(8,128)(2,1)}, bf16[1056,256]{1,0:T(8,128)(2,1)S(1)}, u32[]{:S(2)}, u32[]{:S(2)}) collective-permute-start(bf16[1056,256]{1,0:T(8,128)(2,1)} %get-tuple-element.38), channel_id=1, source_target_pairs={{0,16},{1,17},{2,18},{3,19},{4,20},{5,21},{6,22},{7,23},{8,24},{9,... | collective-permute-start | bytes 1622024 | tf_op jit(solution)/shard_map/ppermute | solution.py:142
  59.3 3.4 %collective-permute-start.36 = (bf16[64,2048]{1,0:T(8,128)(2,1)S(1)}, bf16[64,2048]{1,0:T(8,128)(2,1)}, u32[]{:S(2)}, u32[]{:S(2)}) collective-permute-start(bf16[64,2048]{1,0:T(8,128)(2,1)S(1)} %multiply_convert_fusion.rest_0_), channel_id=1, source_target_pairs={{0,24},{1,25},{2,26},{3,27},{4,28},{5,29},{6,30},{7,31},{8,16},{9,... | collective-permute-start | bytes 786440 | tf_op jit(solution)/shard_map/ppermute | solution.py:142
  62.7 10.5 %collective-permute-done.22.rest_6_ = bf16[1056,256]{1,0:T(8,128)(2,1)S(1)} collective-permute-done((bf16[1056,256]{1,0:T(8,128)(2,1)}, bf16[1056,256]{1,0:T(8,128)(2,1)S(1)}, u32[]{:S(2)}, u32[]{:S(2)}) %collective-permute-start.22) | collective-permute-done | bytes 540704 | tf_op jit(solution)/shard_map/ppermute | solution.py:142
  74.7 18.3 %collective-permute-done.24.rest_8_ = bf16[1056,256]{1,0:T(8,128)(2,1)S(1)} collective-permute-done((bf16[1056,256]{1,0:T(8,128)(2,1)}, bf16[1056,256]{1,0:T(8,128)(2,1)S(1)}, u32[]{:S(2)}, u32[]{:S(2)}) %collective-permute-start.24) | collective-permute-done | bytes 540704 | tf_op jit(solution)/shard_map/ppermute | solution.py:142
  96.4 6.0 %collective-permute-done.43.rest_1_ = bf16[64,2048]{1,0:T(8,128)(2,1)} collective-permute-done((bf16[64,2048]{1,0:T(8,128)(2,1)}, bf16[64,2048]{1,0:T(8,128)(2,1)}, u32[]{:S(2)}, u32[]{:S(2)}) %collective-permute-start.43) | collective-permute-done | bytes 262176 | tf_op jit(solution)/shard_map/ppermute | solution.py:142
  104.7 15.9 %collective-permute-start.37 = (bf16[64,2048]{1,0:T(8,128)(2,1)}, bf16[64,2048]{1,0:T(8,128)(2,1)S(1)}, u32[]{:S(2)}, u32[]{:S(2)}) collective-permute-start(bf16[64,2048]{1,0:T(8,128)(2,1)} %collective-permute-done.36.rest_0_), channel_id=1, source_target_pairs={{0,8},{1,9},{2,10},{3,11},{4,12},{5,13},{6,14},{7,15},{8,0},{9,1},... | collective-permute-start | bytes 786440 | tf_op jit(solution)/shard_map/ppermute | solution.py:142
  120.6 3.6 %ffn.7 = (f32[128,2048]{1,0:T(8,128)S(1)}, bf16[128,2048]{1,0:T(8,128)(2,1)S(1)}) custom-call(s32[8]{0:T(128)S(1)} %stack.35.b_ref, bf16[64,2048]{1,0:T(8,128)(2,1)} %collective-permute-done.36.rest_0_, bf16[64,2048]{1,0:T(8,128)(2,1)} %collective-permute-done.43.rest_1_, bf16[64,2048]{1,0:T(8,128)(2,1)} %collective-permute-done.44.rest_2_, ...), custom_call_target="tpu_custom_call" | custom-call | tf_op jit(solution)/shard_map/ffn/pallas_call | solution.py:275
  124.6 3.3 %collective-permute-start.30 = (bf16[64,2048]{1,0:T(8,128)(2,1)S(1)}, bf16[64,2048]{1,0:T(8,128)(2,1)S(1)}, u32[]{:S(2)}, u32[]{:S(2)}) collective-permute-start(bf16[64,2048]{1,0:T(8,128)(2,1)S(1)} %collective-permute-done.18.rest_1_), channel_id=1, source_target_pairs={{0,8},{1,9},{2,10},{3,11},{4,12},{5,13},{6,14},{7,15},{8,0},{9,1},... | collective-permute-start | bytes 786440 | tf_op jit(solution)/shard_map/ppermute | solution.py:142
  129.6 4.1 %collective-permute-done.29.rest_0_ = bf16[64,2048]{1,0:T(8,128)(2,1)S(1)} collective-permute-done((bf16[64,2048]{1,0:T(8,128)(2,1)S(1)}, bf16[64,2048]{1,0:T(8,128)(2,1)S(1)}, u32[]{:S(2)}, u32[]{:S(2)}) %collective-permute-start.29) | collective-permute-done | bytes 262176 | tf_op jit(solution)/shard_map/ppermute | solution.py:142
  133.6 5.1 %collective-permute-done.30.rest_1_ = bf16[64,2048]{1,0:T(8,128)(2,1)S(1)} collective-permute-done((bf16[64,2048]{1,0:T(8,128)(2,1)S(1)}, bf16[64,2048]{1,0:T(8,128)(2,1)S(1)}, u32[]{:S(2)}, u32[]{:S(2)}) %collective-permute-start.30) | collective-permute-done | bytes 262176 | tf_op jit(solution)/shard_map/ppermute | solution.py:142
  141.8 3.3 %ffn.6 = (f32[128,2048]{1,0:T(8,128)S(1)}, bf16[128,2048]{1,0:T(8,128)(2,1)S(1)}) custom-call(s32[8]{0:T(128)S(1)} %stack.35.b_ref, bf16[64,2048]{1,0:T(8,128)(2,1)S(1)} %collective-permute-done.37.rest_0_, bf16[64,2048]{1,0:T(8,128)(2,1)S(1)} %collective-permute-done.38.rest_1_, bf16[64,2048]{1,0:T(8,128)(2,1)S(1)} %collective-permute-done.39.rest_2_, ...), custom_call_target="tpu_custom_call" | custom-call | tf_op jit(solution)/shard_map/ffn/pallas_call | solution.py:275
  145.2 3.3 %ffn.4 = (f32[128,2048]{1,0:T(8,128)S(1)}, bf16[128,2048]{1,0:T(8,128)(2,1)S(1)}) custom-call(s32[8]{0:T(128)S(1)} %stack.35.b_ref, bf16[64,2048]{1,0:T(8,128)(2,1)S(1)} %copy-done.5, bf16[64,2048]{1,0:T(8,128)(2,1)S(1)} %collective-permute-done.18.rest_1_, bf16[64,2048]{1,0:T(8,128)(2,1)S(1)} %collective-permute-done.19.rest_2_, ...), custom_call_target="tpu_custom_call" | custom-call | tf_op jit(solution)/shard_map/ffn/pallas_call | solution.py:275
  149.1 3.3 %ffn.5 = (f32[128,2048]{1,0:T(8,128)S(1)}, bf16[128,2048]{1,0:T(8,128)(2,1)S(1)}) custom-call(s32[8]{0:T(128)S(1)} %stack.35.b_ref, bf16[64,2048]{1,0:T(8,128)(2,1)S(1)} %collective-permute-done.29.rest_0_, bf16[64,2048]{1,0:T(8,128)(2,1)S(1)} %collective-permute-done.30.rest_1_, bf16[64,2048]{1,0:T(8,128)(2,1)S(1)} %collective-permute-done.31.rest_2_, ...), custom_call_target="tpu_custom_call" | custom-call | tf_op jit(solution)/shard_map/ffn/pallas_call | solution.py:275
  156.7 5.1 %collective-permute-done.48 = bf16[64,2048]{1,0:T(8,128)(2,1)S(1)} collective-permute-done((bf16[64,2048]{1,0:T(8,128)(2,1)S(1)}, bf16[64,2048]{1,0:T(8,128)(2,1)S(1)}, u32[]{:S(2)}, u32[]{:S(2)}) %collective-permute-start.48) | collective-permute-done | bytes 262176 | tf_op jit(solution)/shard_map/ppermute | solution.py:142
  164.6 13.6 %collective-permute-done.34 = bf16[128,2048]{1,0:T(8,128)(2,1)S(1)} collective-permute-done((bf16[128,2048]{1,0:T(8,128)(2,1)S(1)}, bf16[128,2048]{1,0:T(8,128)(2,1)S(1)}, u32[]{:S(2)}, u32[]{:S(2)}) %collective-permute-start.34) | collective-permute-done | bytes 524320 | tf_op jit(solution)/shard_map/ppermute | solution.py:142
  180.1 6.2 %collective-permute-done.35 = bf16[64,2048]{1,0:T(8,128)(2,1)S(1)} collective-permute-done((bf16[64,2048]{1,0:T(8,128)(2,1)S(1)}, bf16[64,2048]{1,0:T(8,128)(2,1)S(1)}, u32[]{:S(2)}, u32[]{:S(2)}) %collective-permute-start.35) | collective-permute-done | bytes 262176 | tf_op jit(solution)/shard_map/ppermute | solution.py:142
  (150 shorter events, 51.3 us)
Async XLA Ops:
  3.2 15.6 %collective-permute-start = (bf16[144,512]{1,0:T(8,128)(2,1)S(1)}, bf16[144,512]{1,0:T(8,128)(2,1)S(1)}, u32[]{:S(2)}, u32[]{:S(2)}) collective-permute-start(bf16[144,512]{1,0:T(8,128)(2,1)S(1)} %maximum_maximum_fusion.rest_0_), channel_id=1, source_target_pairs={{0,8},{1,9},{2,10},{3,11},{4,12},{5,13},{6,14},{7,15},{8,0},{9,1},... | collective-permute-start | bytes 442376 | tf_op jit(solution)/shard_map/ppermute | solution.py:142
  6.3 13.9 %collective-permute-start.1 = (bf16[144,512]{1,0:T(8,128)(2,1)S(1)}, bf16[144,512]{1,0:T(8,128)(2,1)S(1)}, u32[]{:S(2)}, u32[]{:S(2)}) collective-permute-start(bf16[144,512]{1,0:T(8,128)(2,1)S(1)} %maximum_maximum_fusion.rest_0_), channel_id=1, source_target_pairs={{0,16},{1,17},{2,18},{3,19},{4,20},{5,21},{6,22},{7,23},{8,24},{9,... | collective-permute-start | bytes 442376 | tf_op jit(solution)/shard_map/ppermute | solution.py:142
  8.9 12.9 %collective-permute-start.2 = (bf16[144,512]{1,0:T(8,128)(2,1)S(1)}, bf16[144,512]{1,0:T(8,128)(2,1)S(1)}, u32[]{:S(2)}, u32[]{:S(2)}) collective-permute-start(bf16[144,512]{1,0:T(8,128)(2,1)S(1)} %maximum_maximum_fusion.rest_0_), channel_id=1, source_target_pairs={{0,24},{1,25},{2,26},{3,27},{4,28},{5,29},{6,30},{7,31},{8,16},{9,... | collective-permute-start | bytes 442376 | tf_op jit(solution)/shard_map/ppermute | solution.py:142
  8.9 12.9 %collective-permute-start.3 = (bf16[144,512]{1,0:T(8,128)(2,1)S(1)}, bf16[144,512]{1,0:T(8,128)(2,1)S(1)}, u32[]{:S(2)}, u32[]{:S(2)}) collective-permute-start(bf16[144,512]{1,0:T(8,128)(2,1)S(1)} %maximum_maximum_fusion.rest_0_), channel_id=1, source_target_pairs={{0,1},{1,0},{2,3},{3,2},{4,5},{5,4},{6,7},{7,6},{8,9},{9,8},{10,11... | collective-permute-start | bytes 442376 | tf_op jit(solution)/shard_map/ppermute | solution.py:142
  8.9 13.5 %collective-permute-start.7 = (bf16[144,512]{1,0:T(8,128)(2,1)S(1)}, bf16[144,512]{1,0:T(8,128)(2,1)S(1)}, u32[]{:S(2)}, u32[]{:S(2)}) collective-permute-start(bf16[144,512]{1,0:T(8,128)(2,1)S(1)} %maximum_maximum_fusion.rest_0_), channel_id=1, source_target_pairs={{0,4},{1,5},{2,6},{3,7},{4,0},{5,1},{6,2},{7,3},{8,12},{9,13},{10,... | collective-permute-start | bytes 442376 | tf_op jit(solution)/shard_map/ppermute | solution.py:142
  25.7 12.1 %collective-permute-start.11 = (bf16[144,512]{1,0:T(8,128)(2,1)S(1)}, bf16[144,512]{1,0:T(8,128)(2,1)S(1)}, u32[]{:S(2)}, u32[]{:S(2)}) collective-permute-start(bf16[144,512]{1,0:T(8,128)(2,1)S(1)} %collective-permute-done.7.rest_4_), channel_id=1, source_target_pairs={{0,1},{1,0},{2,3},{3,2},{4,5},{5,4},{6,7},{7,6},{8,9},{9,8},{10,11... | collective-permute-start | bytes 442376 | tf_op jit(solution)/shard_map/ppermute | solution.py:142
  45.7 11.7 %collective-permute-start.17 = (bf16[64,2048]{1,0:T(8,128)(2,1)}, bf16[64,2048]{1,0:T(8,128)(2,1)}, u32[]{:S(2)}, u32[]{:S(2)}) collective-permute-start(bf16[64,2048]{1,0:T(8,128)(2,1)} %get-tuple-element.26), channel_id=1, source_target_pairs={{0,3},{1,2},{2,1},{3,0},{4,7},{5,6},{6,5},{7,4},{8,11},{9,10},{10,... | collective-permute-start | bytes 786440 | tf_op jit(solution)/shard_map/ppermute | solution.py:142
  46.9 26.3 %collective-permute-start.22 = (bf16[1056,256]{1,0:T(8,128)(2,1)}, bf16[1056,256]{1,0:T(8,128)(2,1)S(1)}, u32[]{:S(2)}, u32[]{:S(2)}) collective-permute-start(bf16[1056,256]{1,0:T(8,128)(2,1)} %get-tuple-element.39), channel_id=1, source_target_pairs={{0,8},{1,9},{2,10},{3,11},{4,12},{5,13},{6,14},{7,15},{8,0},{9,1},... | collective-permute-start | bytes 1622024 | tf_op jit(solution)/shard_map/ppermute | solution.py:142
  47.3 45.7 %collective-permute-start.24 = (bf16[1056,256]{1,0:T(8,128)(2,1)}, bf16[1056,256]{1,0:T(8,128)(2,1)S(1)}, u32[]{:S(2)}, u32[]{:S(2)}) collective-permute-start(bf16[1056,256]{1,0:T(8,128)(2,1)} %get-tuple-element.38), channel_id=1, source_target_pairs={{0,16},{1,17},{2,18},{3,19},{4,20},{5,21},{6,22},{7,23},{8,24},{9,... | collective-permute-start | bytes 1622024 | tf_op jit(solution)/shard_map/ppermute | solution.py:142
  51.5 42.3 %collective-permute-start.26 = (bf16[1056,256]{1,0:T(8,128)(2,1)}, bf16[1056,256]{1,0:T(8,128)(2,1)S(1)}, u32[]{:S(2)}, u32[]{:S(2)}) collective-permute-start(bf16[1056,256]{1,0:T(8,128)(2,1)} %get-tuple-element.37), channel_id=1, source_target_pairs={{0,24},{1,25},{2,26},{3,27},{4,28},{5,29},{6,30},{7,31},{8,16},{9,... | collective-permute-start | bytes 1622024 | tf_op jit(solution)/shard_map/ppermute | solution.py:142
  54.3 42.1 %collective-permute-start.21 = (bf16[1056,256]{1,0:T(8,128)(2,1)S(1)}, bf16[1056,256]{1,0:T(8,128)(2,1)S(1)}, u32[]{:S(2)}, u32[]{:S(2)}) collective-permute-start(bf16[1056,256]{1,0:T(8,128)(2,1)S(1)} %get-tuple-element.40.rest_4_), channel_id=1, source_target_pairs={{0,4},{1,5},{2,6},{3,7},{4,0},{5,1},{6,2},{7,3},{8,12},{9,13},{10,... | collective-permute-start | bytes 1622024 | tf_op jit(solution)/shard_map/ppermute | solution.py:142
  59.3 35.7 %collective-permute-start.36 = (bf16[64,2048]{1,0:T(8,128)(2,1)S(1)}, bf16[64,2048]{1,0:T(8,128)(2,1)}, u32[]{:S(2)}, u32[]{:S(2)}) collective-permute-start(bf16[64,2048]{1,0:T(8,128)(2,1)S(1)} %multiply_convert_fusion.rest_0_), channel_id=1, source_target_pairs={{0,24},{1,25},{2,26},{3,27},{4,28},{5,29},{6,30},{7,31},{8,16},{9,... | collective-permute-start | bytes 786440 | tf_op jit(solution)/shard_map/ppermute | solution.py:142
  73.3 29.2 %collective-permute-start.23 = (bf16[1056,256]{1,0:T(8,128)(2,1)S(1)}, bf16[1056,256]{1,0:T(8,128)(2,1)}, u32[]{:S(2)}, u32[]{:S(2)}) collective-permute-start(bf16[1056,256]{1,0:T(8,128)(2,1)S(1)} %collective-permute-done.22.rest_6_), channel_id=1, source_target_pairs={{0,4},{1,5},{2,6},{3,7},{4,0},{5,1},{6,2},{7,3},{8,12},{9,13},{10,... | collective-permute-start | bytes 1622024 | tf_op jit(solution)/shard_map/ppermute | solution.py:142
  93.0 11.7 %collective-permute-start.25 = (bf16[1056,256]{1,0:T(8,128)(2,1)S(1)}, bf16[1056,256]{1,0:T(8,128)(2,1)}, u32[]{:S(2)}, u32[]{:S(2)}) collective-permute-start(bf16[1056,256]{1,0:T(8,128)(2,1)S(1)} %collective-permute-done.24.rest_8_), channel_id=1, source_target_pairs={{0,4},{1,5},{2,6},{3,7},{4,0},{5,1},{6,2},{7,3},{8,12},{9,13},{10,... | collective-permute-start | bytes 1622024 | tf_op jit(solution)/shard_map/ppermute | solution.py:142
  93.8 26.8 %collective-permute-start.27 = (bf16[1056,256]{1,0:T(8,128)(2,1)S(1)}, bf16[1056,256]{1,0:T(8,128)(2,1)}, u32[]{:S(2)}, u32[]{:S(2)}) collective-permute-start(bf16[1056,256]{1,0:T(8,128)(2,1)S(1)} %collective-permute-done.26.rest_10_), channel_id=1, source_target_pairs={{0,4},{1,5},{2,6},{3,7},{4,0},{5,1},{6,2},{7,3},{8,12},{9,13},{10,... | collective-permute-start | bytes 1622024 | tf_op jit(solution)/shard_map/ppermute | solution.py:142
  96.4 24.3 %collective-permute-start.44 = (bf16[64,2048]{1,0:T(8,128)(2,1)}, bf16[64,2048]{1,0:T(8,128)(2,1)}, u32[]{:S(2)}, u32[]{:S(2)}) collective-permute-start(bf16[64,2048]{1,0:T(8,128)(2,1)} %collective-permute-done.36.rest_0_), channel_id=1, source_target_pairs={{0,1},{1,0},{2,3},{3,2},{4,5},{5,4},{6,7},{7,6},{8,9},{9,8},{10,11... | collective-permute-start | bytes 786440 | tf_op jit(solution)/shard_map/ppermute | solution.py:142
  102.3 18.3 %collective-permute-start.45 = (bf16[64,2048]{1,0:T(8,128)(2,1)}, bf16[64,2048]{1,0:T(8,128)(2,1)}, u32[]{:S(2)}, u32[]{:S(2)}) collective-permute-start(bf16[64,2048]{1,0:T(8,128)(2,1)} %collective-permute-done.43.rest_1_), channel_id=1, source_target_pairs={{0,1},{1,0},{2,3},{3,2},{4,5},{5,4},{6,7},{7,6},{8,9},{9,8},{10,11... | collective-permute-start | bytes 786440 | tf_op jit(solution)/shard_map/ppermute | solution.py:142
  102.4 22.2 %collective-permute-start.18 = (bf16[64,2048]{1,0:T(8,128)(2,1)}, bf16[64,2048]{1,0:T(8,128)(2,1)S(1)}, u32[]{:S(2)}, u32[]{:S(2)}) collective-permute-start(bf16[64,2048]{1,0:T(8,128)(2,1)} %copy-done.4), channel_id=1, source_target_pairs={{0,2},{1,3},{2,0},{3,1},{4,6},{5,7},{6,4},{7,5},{8,10},{9,11},{10,... | collective-permute-start | bytes 786440 | tf_op jit(solution)/shard_map/ppermute | solution.py:142
  104.7 23.2 %collective-permute-start.37 = (bf16[64,2048]{1,0:T(8,128)(2,1)}, bf16[64,2048]{1,0:T(8,128)(2,1)S(1)}, u32[]{:S(2)}, u32[]{:S(2)}) collective-permute-start(bf16[64,2048]{1,0:T(8,128)(2,1)} %collective-permute-done.36.rest_0_), channel_id=1, source_target_pairs={{0,8},{1,9},{2,10},{3,11},{4,12},{5,13},{6,14},{7,15},{8,0},{9,1},... | collective-permute-start | bytes 786440 | tf_op jit(solution)/shard_map/ppermute | solution.py:142
  124.3 15.1 %collective-permute-start.46 = (bf16[128,2048]{1,0:T(8,128)(2,1)S(1)}, bf16[128,2048]{1,0:T(8,128)(2,1)S(1)}, u32[]{:S(2)}, u32[]{:S(2)}) collective-permute-start(bf16[128,2048]{1,0:T(8,128)(2,1)S(1)} %get-tuple-element.34), channel_id=1, source_target_pairs={{0,1},{1,0},{2,3},{3,2},{4,5},{5,4},{6,7},{7,6},{8,9},{9,8},{10,11... | collective-permute-start | bytes 1572872 | tf_op jit(solution)/shard_map/ppermute | solution.py:142
  124.6 14.2 %collective-permute-start.30 = (bf16[64,2048]{1,0:T(8,128)(2,1)S(1)}, bf16[64,2048]{1,0:T(8,128)(2,1)S(1)}, u32[]{:S(2)}, u32[]{:S(2)}) collective-permute-start(bf16[64,2048]{1,0:T(8,128)(2,1)S(1)} %collective-permute-done.18.rest_1_), channel_id=1, source_target_pairs={{0,8},{1,9},{2,10},{3,11},{4,12},{5,13},{6,14},{7,15},{8,0},{9,1},... | collective-permute-start | bytes 786440 | tf_op jit(solution)/shard_map/ppermute | solution.py:142
  148.5 16.1 %collective-permute-start.28 = (bf16[128,2048]{1,0:T(8,128)(2,1)S(1)}, bf16[128,2048]{1,0:T(8,128)(2,1)S(1)}, u32[]{:S(2)}, u32[]{:S(2)}) collective-permute-start(bf16[128,2048]{1,0:T(8,128)(2,1)S(1)} %get-tuple-element.28), channel_id=1, source_target_pairs={{0,1},{1,0},{2,3},{3,2},{4,5},{5,4},{6,7},{7,6},{8,9},{9,8},{10,11... | collective-permute-start | bytes 1572872 | tf_op jit(solution)/shard_map/ppermute | solution.py:142
  156.4 21.8 %collective-permute-start.34 = (bf16[128,2048]{1,0:T(8,128)(2,1)S(1)}, bf16[128,2048]{1,0:T(8,128)(2,1)S(1)}, u32[]{:S(2)}, u32[]{:S(2)}) collective-permute-start(bf16[128,2048]{1,0:T(8,128)(2,1)S(1)} %add_convert_fusion), channel_id=1, source_target_pairs={{0,8},{1,9},{2,10},{3,11},{4,12},{5,13},{6,14},{7,15},{8,0},{9,1},... | collective-permute-start | bytes 1572872 | tf_op jit(solution)/shard_map/ppermute | solution.py:142
  163.1 17.0 %collective-permute-start.49 = (bf16[64,2048]{1,0:T(8,128)(2,1)S(1)}, bf16[64,2048]{1,0:T(8,128)(2,1)S(1)}, u32[]{:S(2)}, u32[]{:S(2)}) collective-permute-start(bf16[64,2048]{1,0:T(8,128)(2,1)S(1)} %fusion.5), channel_id=1, source_target_pairs={{0,16},{1,17},{2,18},{3,19},{4,20},{5,21},{6,22},{7,23},{8,24},{9,... | collective-permute-start | bytes 786440 | tf_op jit(solution)/shard_map/ppermute | solution.py:142
  (42 other events, 439.0 us)
where the time goes:
time: 188 us; the launch traced here: 187 us
  waiting for transfers between devices  81.7 us (43%)
  starting transfers between devices  60.3 us (32%)
  Pallas kernels  24 us (13%)
  other arithmetic  11 us (6%)
  local copies, waits for them, and re-layouts  7.51 us (4%)
    ppermute x50, waiting for transfers between devices, permute(): return lax.ppermute(value, ('sp', 'tp'), pairs)  81.7 us
    ppermute x50, starting transfers between devices, permute(): return lax.ppermute(value, ('sp', 'tp'), pairs)  60.3 us
    pallas_call x4, Pallas kernels, reduced(): pl.pallas_call(functools.partial(ffn_kernel, len(tokens), nb, fcols), out...  13.6 us
    pallas_call x2, Pallas kernels, attend(): pl.pallas_call(functools.partial(attention_kernel, n, half, first), out_s...  10.4 us
    unnamed x34, local copies, waits for them, and re-layouts  5.08 us
    reduce_sum x3, other arithmetic, normed(): jnp.mean(wide * wide, axis=-1, keepdims=True) + EPS  3.79 us
  transfers between devices with their start and end apart: 50, of which 16 were waited for; matrix products, arithmetic and copies ran while one was open for 8% of the time, Pallas kernels for 10%

commit v1 on v0

--- a/solution.py
+++ b/solution.py
@@ -253,6 +253,11 @@
                 ]
                 + ([] if first else [pltpu.VMEM((tok, width), F32)]),
                 compiler_params=pltpu.CompilerParams(vmem_limit_bytes=small(12 + n)),
+                cost_estimate=pl.CostEstimate(
+                    flops=2 * n * half * wide * (2 * kvr + 3 * tok),
+                    bytes_accessed=2 * n * half * kvr,
+                    transcendentals=n * half * tok * heads,
+                ),
                 name="attention",
             )(t32, q_plain, q_rot, w_key_plain, w_value, *extra, *pieces)
 
@@ -282,6 +287,11 @@
                 out_specs=tuple(vmem(2)),
                 scratch_shapes=[pltpu.VMEM((count, width), BF16)],
                 compiler_params=pltpu.CompilerParams(vmem_limit_bytes=small(14)),
+                cost_estimate=pl.CostEstimate(
+                    flops=6 * count * width * fcols,
+                    bytes_accessed=6 * width * fcols,
+                    transcendentals=count * fcols,
+                ),
                 name="ffn",
             )(blocks, *tokens, *weights)
             return own + permute(other, dc=1).astype(F32)

time: 188 us -> 185 us (0.984)
  local copies, waits for them, and re-layouts: 7.51 us -> 5.08 us
    unnamed x34 -> x38, local copies, waits for them, and re-layouts: 5.08 us -> 3.55 us
  transfers between devices with their start and end apart: 50 -> 50, of which waited for: 16 -> 15; matrix products, arithmetic and copies ran while one was open for 8% -> 8% of each run, Pallas kernels for 10% -> 9%
where the time goes in v1:
time: 185 us; the launch traced here: 184 us
  waiting for transfers between devices  83 us (45%)
  starting transfers between devices  58.5 us (32%)
  Pallas kernels  23.1 us (12%)
  other arithmetic  12.3 us (7%)
  local copies, waits for them, and re-layouts  5.08 us (3%)
    ppermute x50, waiting for transfers between devices, permute(): return lax.ppermute(value, ('sp', 'tp'), pairs)  83 us
    ppermute x50, starting transfers between devices, permute(): return lax.ppermute(value, ('sp', 'tp'), pairs)  58.5 us
    pallas_call x4, Pallas kernels, reduced(): pl.pallas_call(functools.partial(ffn_kernel, len(tokens), nb, fcols), out...  13.6 us
    pallas_call x2, Pallas kernels, attend(): pl.pallas_call(functools.partial(attention_kernel, n, half, first), out_s...  9.49 us
    reduce_sum x3, other arithmetic, normed(): jnp.mean(wide * wide, axis=-1, keepdims=True) + EPS  3.79 us
  transfers between devices with their start and end apart: 50, of which 15 were waited for; matrix products, arithmetic and copies ran while one was open for 8% of the time, Pallas kernels for 9%

profile of v1, /device:TPU:0, one launch (start us, length us, event | category | flops | bytes accessed | tf_op | source)
XLA Modules:
  0.0 184.0 jit_solution(15189390657993018338)
XLA Ops:
  3.2 3.1 %collective-permute-start = (bf16[144,512]{1,0:T(8,128)(2,1)S(1)}, bf16[144,512]{1,0:T(8,128)(2,1)S(1)}, u32[]{:S(2)}, u32[]{:S(2)}) collective-permute-start(bf16[144,512]{1,0:T(8,128)(2,1)S(1)} %maximum_maximum_fusion.rest_0_), channel_id=1, source_target_pairs={{0,8},{1,9},{2,10},{3,11},{4,12},{5,13},{6,14},{7,15},{8,0},{9,1},... | collective-permute-start | bytes 442376 | tf_op jit(solution)/shard_map/ppermute | solution.py:142
  6.3 2.6 %collective-permute-start.1 = (bf16[144,512]{1,0:T(8,128)(2,1)S(1)}, bf16[144,512]{1,0:T(8,128)(2,1)S(1)}, u32[]{:S(2)}, u32[]{:S(2)}) collective-permute-start(bf16[144,512]{1,0:T(8,128)(2,1)S(1)} %maximum_maximum_fusion.rest_0_), channel_id=1, source_target_pairs={{0,16},{1,17},{2,18},{3,19},{4,20},{5,21},{6,22},{7,23},{8,24},{9,... | collective-permute-start | bytes 442376 | tf_op jit(solution)/shard_map/ppermute | solution.py:142
  15.1 2.6 %pad_maximum_fusion = bf16[4,1056,256]{2,1,0:T(8,128)(2,1)} fusion(bf16[4,352,256]{2,1,0:T(8,128)(2,1)} %bitcast.32, bf16[4,352,256]{2,1,0:T(8,128)(2,1)S(1)} %bitcast.31, bf16[4,352,256]{2,1,0:T(8,128)(2,1)S(1)} %bitcast.30), kind=kLoop, calls=%fused_computation | loop fusion | flops 6488064 | bytes 4325376 | tf_op jit(solution)/shard_map/concatenate | solution.py:195
  27.0 3.2 %collective-permute-done.9.rest_6_ = bf16[144,512]{1,0:T(8,128)(2,1)S(1)} collective-permute-done((bf16[144,512]{1,0:T(8,128)(2,1)S(1)}, bf16[144,512]{1,0:T(8,128)(2,1)S(1)}, u32[]{:S(2)}, u32[]{:S(2)}) %collective-permute-start.9) | collective-permute-done | bytes 147488 | tf_op jit(solution)/shard_map/ppermute | solution.py:142
  30.2 2.5 %collective-permute-done.10.rest_7_ = bf16[144,512]{1,0:T(8,128)(2,1)S(1)} collective-permute-done((bf16[144,512]{1,0:T(8,128)(2,1)S(1)}, bf16[144,512]{1,0:T(8,128)(2,1)S(1)}, u32[]{:S(2)}, u32[]{:S(2)}) %collective-permute-start.10) | collective-permute-done | bytes 147488 | tf_op jit(solution)/shard_map/ppermute | solution.py:142
  32.7 3.8 %attention.2 = (f32[256,512]{1,0:T(8,128)S(1)}, f32[256,512]{1,0:T(8,128)S(1)}, f32[256,512]{1,0:T(8,128)S(1)}) custom-call(s32[1]{0:T(128)} %bitcast.t_ref, bf16[256,512]{1,0:T(8,128)(2,1)S(1)} %convolution_convert_fusion.qp_ref, bf16[256,256]{1,0:T(8,128)(2,1)S(1)} %copy.23.qr_ref, bf16[512,512]{1,0:T(8,128)(2,1)S(1)} %copy-done.5, ...), custom_call_target="tpu_custom_call" | custom-call | flops 1879048192 | bytes 1048576 | tf_op jit(solution)/shard_map/attention/pallas_call | solution.py:243
  36.6 5.7 %attention.3 = (f32[64,2048]{1,0:T(8,128)S(1)}, bf16[64,2048]{1,0:T(8,128)(2,1)S(1)}, bf16[64,2048]{1,0:T(8,128)(2,1)S(1)}, bf16[64,2048]{1,0:T(8,128)(2,1)}) custom-call(s32[1]{0:T(128)} %bitcast.t_ref, bf16[256,512]{1,0:T(8,128)(2,1)S(1)} %convolution_convert_fusion.qp_ref, bf16[256,256]{1,0:T(8,128)(2,1)S(1)} %copy.23.qr_ref, ...), custom_call_target="tpu_custom_call" | custom-call | flops 1879048192 | bytes 1048576 | tf_op jit(solution)/shard_map/attention/pallas_call | solution.py:243
  46.2 3.5 %collective-permute-start.24 = (bf16[1056,256]{1,0:T(8,128)(2,1)}, bf16[1056,256]{1,0:T(8,128)(2,1)S(1)}, u32[]{:S(2)}, u32[]{:S(2)}) collective-permute-start(bf16[1056,256]{1,0:T(8,128)(2,1)} %get-tuple-element.38), channel_id=1, source_target_pairs={{0,16},{1,17},{2,18},{3,19},{4,20},{5,21},{6,22},{7,23},{8,24},{9,... | collective-permute-start | bytes 1622024 | tf_op jit(solution)/shard_map/ppermute | solution.py:142
  52.6 3.2 %collective-permute-done.17 = bf16[64,2048]{1,0:T(8,128)(2,1)} collective-permute-done((bf16[64,2048]{1,0:T(8,128)(2,1)}, bf16[64,2048]{1,0:T(8,128)(2,1)}, u32[]{:S(2)}, u32[]{:S(2)}) %collective-permute-start.17) | collective-permute-done | bytes 262176 | tf_op jit(solution)/shard_map/ppermute | solution.py:142
  57.7 3.6 %collective-permute-start.36 = (bf16[64,2048]{1,0:T(8,128)(2,1)S(1)}, bf16[64,2048]{1,0:T(8,128)(2,1)}, u32[]{:S(2)}, u32[]{:S(2)}) collective-permute-start(bf16[64,2048]{1,0:T(8,128)(2,1)S(1)} %multiply_convert_fusion.rest_0_), channel_id=1, source_target_pairs={{0,24},{1,25},{2,26},{3,27},{4,28},{5,29},{6,30},{7,31},{8,16},{9,... | collective-permute-start | bytes 786440 | tf_op jit(solution)/shard_map/ppermute | solution.py:142
  61.4 10.5 %collective-permute-done.22.rest_6_ = bf16[1056,256]{1,0:T(8,128)(2,1)S(1)} collective-permute-done((bf16[1056,256]{1,0:T(8,128)(2,1)}, bf16[1056,256]{1,0:T(8,128)(2,1)S(1)}, u32[]{:S(2)}, u32[]{:S(2)}) %collective-permute-start.22) | collective-permute-done | bytes 540704 | tf_op jit(solution)/shard_map/ppermute | solution.py:142
  72.4 19.4 %collective-permute-done.24.rest_8_ = bf16[1056,256]{1,0:T(8,128)(2,1)S(1)} collective-permute-done((bf16[1056,256]{1,0:T(8,128)(2,1)}, bf16[1056,256]{1,0:T(8,128)(2,1)S(1)}, u32[]{:S(2)}, u32[]{:S(2)}) %collective-permute-start.24) | collective-permute-done | bytes 540704 | tf_op jit(solution)/shard_map/ppermute | solution.py:142
  95.3 5.9 %collective-permute-done.43.rest_1_ = bf16[64,2048]{1,0:T(8,128)(2,1)} collective-permute-done((bf16[64,2048]{1,0:T(8,128)(2,1)}, bf16[64,2048]{1,0:T(8,128)(2,1)}, u32[]{:S(2)}, u32[]{:S(2)}) %collective-permute-start.43) | collective-permute-done | bytes 262176 | tf_op jit(solution)/shard_map/ppermute | solution.py:142
  103.3 16.2 %collective-permute-start.37 = (bf16[64,2048]{1,0:T(8,128)(2,1)}, bf16[64,2048]{1,0:T(8,128)(2,1)S(1)}, u32[]{:S(2)}, u32[]{:S(2)}) collective-permute-start(bf16[64,2048]{1,0:T(8,128)(2,1)} %collective-permute-done.36.rest_0_), channel_id=1, source_target_pairs={{0,8},{1,9},{2,10},{3,11},{4,12},{5,13},{6,14},{7,15},{8,0},{9,1},... | collective-permute-start | bytes 786440 | tf_op jit(solution)/shard_map/ppermute | solution.py:142
  119.5 3.6 %ffn.7 = (f32[128,2048]{1,0:T(8,128)S(1)}, bf16[128,2048]{1,0:T(8,128)(2,1)S(1)}) custom-call(s32[8]{0:T(128)S(1)} %stack.35.b_ref, bf16[64,2048]{1,0:T(8,128)(2,1)} %collective-permute-done.36.rest_0_, bf16[64,2048]{1,0:T(8,128)(2,1)} %collective-permute-done.43.rest_1_, bf16[64,2048]{1,0:T(8,128)(2,1)} %collective-permute-done.44.rest_2_, ...), custom_call_target="tpu_custom_call" | custom-call | flops 1107296256 | bytes 4325376 | tf_op jit(solution)/shard_map/ffn/pallas_call | solution.py:280
  123.8 3.0 %collective-permute-start.30 = (bf16[64,2048]{1,0:T(8,128)(2,1)S(1)}, bf16[64,2048]{1,0:T(8,128)(2,1)S(1)}, u32[]{:S(2)}, u32[]{:S(2)}) collective-permute-start(bf16[64,2048]{1,0:T(8,128)(2,1)S(1)} %collective-permute-done.18.rest_1_), channel_id=1, source_target_pairs={{0,8},{1,9},{2,10},{3,11},{4,12},{5,13},{6,14},{7,15},{8,0},{9,1},... | collective-permute-start | bytes 786440 | tf_op jit(solution)/shard_map/ppermute | solution.py:142
  128.4 4.5 %collective-permute-done.29.rest_0_ = bf16[64,2048]{1,0:T(8,128)(2,1)S(1)} collective-permute-done((bf16[64,2048]{1,0:T(8,128)(2,1)S(1)}, bf16[64,2048]{1,0:T(8,128)(2,1)S(1)}, u32[]{:S(2)}, u32[]{:S(2)}) %collective-permute-start.29) | collective-permute-done | bytes 262176 | tf_op jit(solution)/shard_map/ppermute | solution.py:142
  132.9 4.7 %collective-permute-done.30.rest_1_ = bf16[64,2048]{1,0:T(8,128)(2,1)S(1)} collective-permute-done((bf16[64,2048]{1,0:T(8,128)(2,1)S(1)}, bf16[64,2048]{1,0:T(8,128)(2,1)S(1)}, u32[]{:S(2)}, u32[]{:S(2)}) %collective-permute-start.30) | collective-permute-done | bytes 262176 | tf_op jit(solution)/shard_map/ppermute | solution.py:142
  138.9 3.3 %ffn.4 = (f32[128,2048]{1,0:T(8,128)S(1)}, bf16[128,2048]{1,0:T(8,128)(2,1)S(1)}) custom-call(s32[8]{0:T(128)S(1)} %stack.35.b_ref, bf16[64,2048]{1,0:T(8,128)(2,1)S(1)} %copy-done.2, bf16[64,2048]{1,0:T(8,128)(2,1)S(1)} %collective-permute-done.18.rest_1_, bf16[64,2048]{1,0:T(8,128)(2,1)S(1)} %collective-permute-done.19.rest_2_, ...), custom_call_target="tpu_custom_call" | custom-call | flops 1107296256 | bytes 4325376 | tf_op jit(solution)/shard_map/ffn/pallas_call | solution.py:280
  142.4 3.3 %ffn.6 = (f32[128,2048]{1,0:T(8,128)S(1)}, bf16[128,2048]{1,0:T(8,128)(2,1)S(1)}) custom-call(s32[8]{0:T(128)S(1)} %stack.35.b_ref, bf16[64,2048]{1,0:T(8,128)(2,1)S(1)} %collective-permute-done.37.rest_0_, bf16[64,2048]{1,0:T(8,128)(2,1)S(1)} %collective-permute-done.38.rest_1_, bf16[64,2048]{1,0:T(8,128)(2,1)S(1)} %collective-permute-done.39.rest_2_, ...), custom_call_target="tpu_custom_call" | custom-call | flops 1107296256 | bytes 4325376 | tf_op jit(solution)/shard_map/ffn/pallas_call | solution.py:280
  146.2 3.3 %ffn.5 = (f32[128,2048]{1,0:T(8,128)S(1)}, bf16[128,2048]{1,0:T(8,128)(2,1)S(1)}) custom-call(s32[8]{0:T(128)S(1)} %stack.35.b_ref, bf16[64,2048]{1,0:T(8,128)(2,1)S(1)} %collective-permute-done.29.rest_0_, bf16[64,2048]{1,0:T(8,128)(2,1)S(1)} %collective-permute-done.30.rest_1_, bf16[64,2048]{1,0:T(8,128)(2,1)S(1)} %collective-permute-done.31.rest_2_, ...), custom_call_target="tpu_custom_call" | custom-call | flops 1107296256 | bytes 4325376 | tf_op jit(solution)/shard_map/ffn/pallas_call | solution.py:280
  153.9 5.2 %collective-permute-done.48 = bf16[64,2048]{1,0:T(8,128)(2,1)S(1)} collective-permute-done((bf16[64,2048]{1,0:T(8,128)(2,1)S(1)}, bf16[64,2048]{1,0:T(8,128)(2,1)S(1)}, u32[]{:S(2)}, u32[]{:S(2)}) %collective-permute-start.48) | collective-permute-done | bytes 262176 | tf_op jit(solution)/shard_map/ppermute | solution.py:142
  161.8 13.4 %collective-permute-done.34 = bf16[128,2048]{1,0:T(8,128)(2,1)S(1)} collective-permute-done((bf16[128,2048]{1,0:T(8,128)(2,1)S(1)}, bf16[128,2048]{1,0:T(8,128)(2,1)S(1)}, u32[]{:S(2)}, u32[]{:S(2)}) %collective-permute-start.34) | collective-permute-done | bytes 524320 | tf_op jit(solution)/shard_map/ppermute | solution.py:142
  177.1 6.1 %collective-permute-done.35 = bf16[64,2048]{1,0:T(8,128)(2,1)S(1)} collective-permute-done((bf16[64,2048]{1,0:T(8,128)(2,1)S(1)}, bf16[64,2048]{1,0:T(8,128)(2,1)S(1)}, u32[]{:S(2)}, u32[]{:S(2)}) %collective-permute-start.35) | collective-permute-done | bytes 262176 | tf_op jit(solution)/shard_map/ppermute | solution.py:142
  (154 shorter events, 47.2 us)
Async XLA Ops:
  3.2 15.1 %collective-permute-start = (bf16[144,512]{1,0:T(8,128)(2,1)S(1)}, bf16[144,512]{1,0:T(8,128)(2,1)S(1)}, u32[]{:S(2)}, u32[]{:S(2)}) collective-permute-start(bf16[144,512]{1,0:T(8,128)(2,1)S(1)} %maximum_maximum_fusion.rest_0_), channel_id=1, source_target_pairs={{0,8},{1,9},{2,10},{3,11},{4,12},{5,13},{6,14},{7,15},{8,0},{9,1},... | collective-permute-start | bytes 442376 | tf_op jit(solution)/shard_map/ppermute | solution.py:142
  6.3 13.9 %collective-permute-start.1 = (bf16[144,512]{1,0:T(8,128)(2,1)S(1)}, bf16[144,512]{1,0:T(8,128)(2,1)S(1)}, u32[]{:S(2)}, u32[]{:S(2)}) collective-permute-start(bf16[144,512]{1,0:T(8,128)(2,1)S(1)} %maximum_maximum_fusion.rest_0_), channel_id=1, source_target_pairs={{0,16},{1,17},{2,18},{3,19},{4,20},{5,21},{6,22},{7,23},{8,24},{9,... | collective-permute-start | bytes 442376 | tf_op jit(solution)/shard_map/ppermute | solution.py:142
  8.9 12.9 %collective-permute-start.2 = (bf16[144,512]{1,0:T(8,128)(2,1)S(1)}, bf16[144,512]{1,0:T(8,128)(2,1)S(1)}, u32[]{:S(2)}, u32[]{:S(2)}) collective-permute-start(bf16[144,512]{1,0:T(8,128)(2,1)S(1)} %maximum_maximum_fusion.rest_0_), channel_id=1, source_target_pairs={{0,24},{1,25},{2,26},{3,27},{4,28},{5,29},{6,30},{7,31},{8,16},{9,... | collective-permute-start | bytes 442376 | tf_op jit(solution)/shard_map/ppermute | solution.py:142
  8.9 12.9 %collective-permute-start.3 = (bf16[144,512]{1,0:T(8,128)(2,1)S(1)}, bf16[144,512]{1,0:T(8,128)(2,1)S(1)}, u32[]{:S(2)}, u32[]{:S(2)}) collective-permute-start(bf16[144,512]{1,0:T(8,128)(2,1)S(1)} %maximum_maximum_fusion.rest_0_), channel_id=1, source_target_pairs={{0,1},{1,0},{2,3},{3,2},{4,5},{5,4},{6,7},{7,6},{8,9},{9,8},{10,11... | collective-permute-start | bytes 442376 | tf_op jit(solution)/shard_map/ppermute | solution.py:142
  8.9 13.5 %collective-permute-start.7 = (bf16[144,512]{1,0:T(8,128)(2,1)S(1)}, bf16[144,512]{1,0:T(8,128)(2,1)S(1)}, u32[]{:S(2)}, u32[]{:S(2)}) collective-permute-start(bf16[144,512]{1,0:T(8,128)(2,1)S(1)} %maximum_maximum_fusion.rest_0_), channel_id=1, source_target_pairs={{0,4},{1,5},{2,6},{3,7},{4,0},{5,1},{6,2},{7,3},{8,12},{9,13},{10,... | collective-permute-start | bytes 442376 | tf_op jit(solution)/shard_map/ppermute | solution.py:142
  44.3 11.5 %collective-permute-start.17 = (bf16[64,2048]{1,0:T(8,128)(2,1)}, bf16[64,2048]{1,0:T(8,128)(2,1)}, u32[]{:S(2)}, u32[]{:S(2)}) collective-permute-start(bf16[64,2048]{1,0:T(8,128)(2,1)} %get-tuple-element.26), channel_id=1, source_target_pairs={{0,3},{1,2},{2,1},{3,0},{4,7},{5,6},{6,5},{7,4},{8,11},{9,10},{10,... | collective-permute-start | bytes 786440 | tf_op jit(solution)/shard_map/ppermute | solution.py:142
  45.5 26.3 %collective-permute-start.22 = (bf16[1056,256]{1,0:T(8,128)(2,1)}, bf16[1056,256]{1,0:T(8,128)(2,1)S(1)}, u32[]{:S(2)}, u32[]{:S(2)}) collective-permute-start(bf16[1056,256]{1,0:T(8,128)(2,1)} %get-tuple-element.39), channel_id=1, source_target_pairs={{0,8},{1,9},{2,10},{3,11},{4,12},{5,13},{6,14},{7,15},{8,0},{9,1},... | collective-permute-start | bytes 1622024 | tf_op jit(solution)/shard_map/ppermute | solution.py:142
  46.2 45.6 %collective-permute-start.24 = (bf16[1056,256]{1,0:T(8,128)(2,1)}, bf16[1056,256]{1,0:T(8,128)(2,1)S(1)}, u32[]{:S(2)}, u32[]{:S(2)}) collective-permute-start(bf16[1056,256]{1,0:T(8,128)(2,1)} %get-tuple-element.38), channel_id=1, source_target_pairs={{0,16},{1,17},{2,18},{3,19},{4,20},{5,21},{6,22},{7,23},{8,24},{9,... | collective-permute-start | bytes 1622024 | tf_op jit(solution)/shard_map/ppermute | solution.py:142
  50.4 42.0 %collective-permute-start.26 = (bf16[1056,256]{1,0:T(8,128)(2,1)}, bf16[1056,256]{1,0:T(8,128)(2,1)S(1)}, u32[]{:S(2)}, u32[]{:S(2)}) collective-permute-start(bf16[1056,256]{1,0:T(8,128)(2,1)} %get-tuple-element.37), channel_id=1, source_target_pairs={{0,24},{1,25},{2,26},{3,27},{4,28},{5,29},{6,30},{7,31},{8,16},{9,... | collective-permute-start | bytes 1622024 | tf_op jit(solution)/shard_map/ppermute | solution.py:142
  52.0 43.2 %collective-permute-start.21 = (bf16[1056,256]{1,0:T(8,128)(2,1)S(1)}, bf16[1056,256]{1,0:T(8,128)(2,1)S(1)}, u32[]{:S(2)}, u32[]{:S(2)}) collective-permute-start(bf16[1056,256]{1,0:T(8,128)(2,1)S(1)} %get-tuple-element.40.rest_4_), channel_id=1, source_target_pairs={{0,4},{1,5},{2,6},{3,7},{4,0},{5,1},{6,2},{7,3},{8,12},{9,13},{10,... | collective-permute-start | bytes 1622024 | tf_op jit(solution)/shard_map/ppermute | solution.py:142
  57.7 36.1 %collective-permute-start.36 = (bf16[64,2048]{1,0:T(8,128)(2,1)S(1)}, bf16[64,2048]{1,0:T(8,128)(2,1)}, u32[]{:S(2)}, u32[]{:S(2)}) collective-permute-start(bf16[64,2048]{1,0:T(8,128)(2,1)S(1)} %multiply_convert_fusion.rest_0_), channel_id=1, source_target_pairs={{0,24},{1,25},{2,26},{3,27},{4,28},{5,29},{6,30},{7,31},{8,16},{9,... | collective-permute-start | bytes 786440 | tf_op jit(solution)/shard_map/ppermute | solution.py:142
  71.8 29.4 %collective-permute-start.23 = (bf16[1056,256]{1,0:T(8,128)(2,1)S(1)}, bf16[1056,256]{1,0:T(8,128)(2,1)}, u32[]{:S(2)}, u32[]{:S(2)}) collective-permute-start(bf16[1056,256]{1,0:T(8,128)(2,1)S(1)} %collective-permute-done.22.rest_6_), channel_id=1, source_target_pairs={{0,4},{1,5},{2,6},{3,7},{4,0},{5,1},{6,2},{7,3},{8,12},{9,13},{10,... | collective-permute-start | bytes 1622024 | tf_op jit(solution)/shard_map/ppermute | solution.py:142
  91.8 11.4 %collective-permute-start.25 = (bf16[1056,256]{1,0:T(8,128)(2,1)S(1)}, bf16[1056,256]{1,0:T(8,128)(2,1)}, u32[]{:S(2)}, u32[]{:S(2)}) collective-permute-start(bf16[1056,256]{1,0:T(8,128)(2,1)S(1)} %collective-permute-done.24.rest_8_), channel_id=1, source_target_pairs={{0,4},{1,5},{2,6},{3,7},{4,0},{5,1},{6,2},{7,3},{8,12},{9,13},{10,... | collective-permute-start | bytes 1622024 | tf_op jit(solution)/shard_map/ppermute | solution.py:142
  92.4 27.1 %collective-permute-start.27 = (bf16[1056,256]{1,0:T(8,128)(2,1)S(1)}, bf16[1056,256]{1,0:T(8,128)(2,1)}, u32[]{:S(2)}, u32[]{:S(2)}) collective-permute-start(bf16[1056,256]{1,0:T(8,128)(2,1)S(1)} %collective-permute-done.26.rest_10_), channel_id=1, source_target_pairs={{0,4},{1,5},{2,6},{3,7},{4,0},{5,1},{6,2},{7,3},{8,12},{9,13},{10,... | collective-permute-start | bytes 1622024 | tf_op jit(solution)/shard_map/ppermute | solution.py:142
  95.3 24.2 %collective-permute-start.44 = (bf16[64,2048]{1,0:T(8,128)(2,1)}, bf16[64,2048]{1,0:T(8,128)(2,1)}, u32[]{:S(2)}, u32[]{:S(2)}) collective-permute-start(bf16[64,2048]{1,0:T(8,128)(2,1)} %collective-permute-done.36.rest_0_), channel_id=1, source_target_pairs={{0,1},{1,0},{2,3},{3,2},{4,5},{5,4},{6,7},{7,6},{8,9},{9,8},{10,11... | collective-permute-start | bytes 786440 | tf_op jit(solution)/shard_map/ppermute | solution.py:142
  101.2 18.3 %collective-permute-start.45 = (bf16[64,2048]{1,0:T(8,128)(2,1)}, bf16[64,2048]{1,0:T(8,128)(2,1)}, u32[]{:S(2)}, u32[]{:S(2)}) collective-permute-start(bf16[64,2048]{1,0:T(8,128)(2,1)} %collective-permute-done.43.rest_1_), channel_id=1, source_target_pairs={{0,1},{1,0},{2,3},{3,2},{4,5},{5,4},{6,7},{7,6},{8,9},{9,8},{10,11... | collective-permute-start | bytes 786440 | tf_op jit(solution)/shard_map/ppermute | solution.py:142
  101.3 22.5 %collective-permute-start.18 = (bf16[64,2048]{1,0:T(8,128)(2,1)}, bf16[64,2048]{1,0:T(8,128)(2,1)S(1)}, u32[]{:S(2)}, u32[]{:S(2)}) collective-permute-start(bf16[64,2048]{1,0:T(8,128)(2,1)} %copy-done.1), channel_id=1, source_target_pairs={{0,2},{1,3},{2,0},{3,1},{4,6},{5,7},{6,4},{7,5},{8,10},{9,11},{10,... | collective-permute-start | bytes 786440 | tf_op jit(solution)/shard_map/ppermute | solution.py:142
  103.3 23.5 %collective-permute-start.37 = (bf16[64,2048]{1,0:T(8,128)(2,1)}, bf16[64,2048]{1,0:T(8,128)(2,1)S(1)}, u32[]{:S(2)}, u32[]{:S(2)}) collective-permute-start(bf16[64,2048]{1,0:T(8,128)(2,1)} %collective-permute-done.36.rest_0_), channel_id=1, source_target_pairs={{0,8},{1,9},{2,10},{3,11},{4,12},{5,13},{6,14},{7,15},{8,0},{9,1},... | collective-permute-start | bytes 786440 | tf_op jit(solution)/shard_map/ppermute | solution.py:142
  123.1 15.0 %collective-permute-start.46 = (bf16[128,2048]{1,0:T(8,128)(2,1)S(1)}, bf16[128,2048]{1,0:T(8,128)(2,1)S(1)}, u32[]{:S(2)}, u32[]{:S(2)}) collective-permute-start(bf16[128,2048]{1,0:T(8,128)(2,1)S(1)} %get-tuple-element.34), channel_id=1, source_target_pairs={{0,1},{1,0},{2,3},{3,2},{4,5},{5,4},{6,7},{7,6},{8,9},{9,8},{10,11... | collective-permute-start | bytes 1572872 | tf_op jit(solution)/shard_map/ppermute | solution.py:142
  123.8 13.8 %collective-permute-start.30 = (bf16[64,2048]{1,0:T(8,128)(2,1)S(1)}, bf16[64,2048]{1,0:T(8,128)(2,1)S(1)}, u32[]{:S(2)}, u32[]{:S(2)}) collective-permute-start(bf16[64,2048]{1,0:T(8,128)(2,1)S(1)} %collective-permute-done.18.rest_1_), channel_id=1, source_target_pairs={{0,8},{1,9},{2,10},{3,11},{4,12},{5,13},{6,14},{7,15},{8,0},{9,1},... | collective-permute-start | bytes 786440 | tf_op jit(solution)/shard_map/ppermute | solution.py:142
  132.9 13.3 %collective-permute-start.31 = (bf16[64,2048]{1,0:T(8,128)(2,1)S(1)}, bf16[64,2048]{1,0:T(8,128)(2,1)S(1)}, u32[]{:S(2)}, u32[]{:S(2)}) collective-permute-start(bf16[64,2048]{1,0:T(8,128)(2,1)S(1)} %collective-permute-done.29.rest_0_), channel_id=1, source_target_pairs={{0,1},{1,0},{2,3},{3,2},{4,5},{5,4},{6,7},{7,6},{8,9},{9,8},{10,11... | collective-permute-start | bytes 786440 | tf_op jit(solution)/shard_map/ppermute | solution.py:142
  142.2 19.6 %collective-permute-start.28 = (bf16[128,2048]{1,0:T(8,128)(2,1)S(1)}, bf16[128,2048]{1,0:T(8,128)(2,1)S(1)}, u32[]{:S(2)}, u32[]{:S(2)}) collective-permute-start(bf16[128,2048]{1,0:T(8,128)(2,1)S(1)} %get-tuple-element.28), channel_id=1, source_target_pairs={{0,1},{1,0},{2,3},{3,2},{4,5},{5,4},{6,7},{7,6},{8,9},{9,8},{10,11... | collective-permute-start | bytes 1572872 | tf_op jit(solution)/shard_map/ppermute | solution.py:142
  153.5 21.7 %collective-permute-start.34 = (bf16[128,2048]{1,0:T(8,128)(2,1)S(1)}, bf16[128,2048]{1,0:T(8,128)(2,1)S(1)}, u32[]{:S(2)}, u32[]{:S(2)}) collective-permute-start(bf16[128,2048]{1,0:T(8,128)(2,1)S(1)} %add_convert_fusion), channel_id=1, source_target_pairs={{0,8},{1,9},{2,10},{3,11},{4,12},{5,13},{6,14},{7,15},{8,0},{9,1},... | collective-permute-start | bytes 1572872 | tf_op jit(solution)/shard_map/ppermute | solution.py:142
  160.2 17.0 %collective-permute-start.49 = (bf16[64,2048]{1,0:T(8,128)(2,1)S(1)}, bf16[64,2048]{1,0:T(8,128)(2,1)S(1)}, u32[]{:S(2)}, u32[]{:S(2)}) collective-permute-start(bf16[64,2048]{1,0:T(8,128)(2,1)S(1)} %fusion.5), channel_id=1, source_target_pairs={{0,16},{1,17},{2,18},{3,19},{4,20},{5,21},{6,22},{7,23},{8,24},{9,... | collective-permute-start | bytes 786440 | tf_op jit(solution)/shard_map/ppermute | solution.py:142
  (44 other events, 415.4 us)
